TPU v7x, 32 devices: a whole 2x2x4 slice. The times are simulated.
32 devices in a mesh: sp: 8 (over z, y), tp: 4 (over x, core).
Axes of the slice: x: 2, y: 2, z: 4, core: 2. Of those that a mesh axis runs over, the one named last changes fastest.
Arguments:
- tokens: bfloat16 [1024, 2048], P(('sp', 'tp')), may hold values from -6 to 6
- norm_gain: float32 [2048], replicated, may hold values from 0.1 to 1.9
- w_filter_b: bfloat16 [2048, 1024], P('sp', 'tp'), may hold values from -0.125 to 0.125
- w_filter_c: bfloat16 [2048, 1024], P('sp', 'tp'), may hold values from -0.125 to 0.125
- w_filter_v: bfloat16 [2048, 1024], P('sp', 'tp'), may hold values from -0.125 to 0.125
- filter_taps: float32 [3, 1024], P(None, 'tp'), may hold values from -3.5 to 3.5
- w_query: bfloat16 [2048, 1024], P('sp', 'tp'), may hold values from -0.125 to 0.125
- retention_gate_matrix: bfloat16 [2048, 1024], P('sp', 'tp'), may hold values from -0.125 to 0.125
- w_input: bfloat16 [2048, 1024], P('sp', 'tp'), may hold values from -0.125 to 0.125
- forget_gap: float32 [1024], P('tp'), may hold values from 0 to 0.12
- additive_fade_log: float32 [1024, 1024], P('sp', 'tp'), may hold values from -1.1 to 0
- head_gain: float32 [128], replicated, may hold values from 0.1 to 1.9
- initial_state: float32 [8, 128, 128], P('tp'), may hold values from -0.0546875 to 0.0546875
- w_out_filter: bfloat16 [1024, 2048], P('tp'), may hold values from -0.125 to 0.125
- w_out_rec: bfloat16 [1024, 2048], P('tp'), may hold values from -0.125 to 0.125
Outputs:
- mixed: bfloat16 [1024, 2048], P(('sp', 'tp'))
All inputs are finite; a program needn't handle non-finite values.
Results may differ from a plain program's by a relative error of at most 0.03.
Values may be sent and summed in bfloat16 or wider, within the bound.
A program may use at most 64 MiB of HBM per device.

v0:
```python
import jax
import jax.numpy as jnp
from jax import lax
from jax.sharding import PartitionSpec as P

HEAD_DIM = 128
SPAN = 64
TAPS = 3


epsilon = 1e-06
highest_precision = lax.Precision.HIGHEST


def shifted(block, axis, distance):
    devices = range(lax.axis_size(axis))
    route = [(i - distance, i) for i in devices if i - distance in devices]
    return lax.ppermute(block, axis, route)


def prefix(x, axis, join, neutral):
    place = lax.axis_index(axis)
    gathered = jax.tree.map(
        lambda a, kind: lax.all_gather(a.astype(kind), axis), x, (jnp.bfloat16, jnp.bfloat16)
    )
    state = jax.tree.map(lambda a, e: jnp.zeros_like(a) + jnp.asarray(e, a.dtype), x, neutral)

    def one(step, state):
        return join(
            state,
            jax.tree.map(
                lambda a, own: lax.dynamic_index_in_dim(a, step, 0, False).astype(own.dtype),
                gathered,
                x,
            ),
        )

    return lax.fori_loop(0, place, one, state)


def project(normed, weight):
    return jnp.dot(normed, weight, preferred_element_type=jnp.float32).astype(jnp.bfloat16)


def block_step(carried_state, inputs):
    block_query, block_key, block_value_rows, block_decay = inputs
    causal = jnp.tril(jnp.ones((SPAN, SPAN), dtype=bool))
    running = jnp.cumsum(block_decay, axis=0)
    scaled_query = block_query * jnp.exp(running)
    key_scaled = block_key * jnp.exp(-running)
    scores = jnp.einsum("thk,shk->hts", scaled_query, key_scaled, precision=highest_precision)
    scores = jnp.where(causal[None], scores, 0.0)
    final_result = jnp.einsum("hts,shv->thv", scores, block_value_rows, precision=highest_precision)
    final_result = final_result + jnp.einsum(
        "oql,qlz->oqz", scaled_query, carried_state, precision=highest_precision
    )
    final_state = running[-1]
    key_remainder = block_key * jnp.exp(final_state[None] - running)
    updated_state = jnp.exp(final_state)[:, :, None] * carried_state + jnp.einsum(
        "dri,drz->riz", key_remainder, block_value_rows, precision=highest_precision
    )
    return (updated_state, final_result)


def local_recurrence(normed, weights, forget_gap, additive_fade_log):
    queries = project(normed, weights[0]).astype(jnp.float32)
    forget_logit = project(normed, weights[1]).astype(jnp.float32)
    input_value = project(normed, weights[2]).astype(jnp.float32)
    key_rate = forget_gap * jax.nn.sigmoid(-forget_logit)
    log_decay = jnp.log1p(-key_rate) + additive_fade_log
    value_in = jax.nn.silu(input_value)
    length = queries.shape[0]
    head_count = queries.shape[1] // HEAD_DIM

    def heads_blocks(flat_rows):
        return flat_rows.reshape(length // SPAN, SPAN, head_count, HEAD_DIM)

    start_state = jnp.zeros((head_count, HEAD_DIM, HEAD_DIM), jnp.float32)
    end_state, within_block = lax.scan(
        block_step,
        start_state,
        (
            heads_blocks(queries),
            heads_blocks(key_rate),
            heads_blocks(value_in),
            heads_blocks(log_decay),
        ),
    )
    running = jnp.cumsum(log_decay.reshape(length, head_count, HEAD_DIM), axis=0)
    scaled_query = queries.reshape(length, head_count, HEAD_DIM) * jnp.exp(running)
    return (
        within_block.reshape(length, head_count, HEAD_DIM),
        scaled_query,
        running[-1],
        end_state,
    )


def chain_combine(earlier, later):
    return (earlier[0] + later[0], jnp.exp(later[0])[:, :, None] * earlier[1] + later[1])


def body(
    tokens,
    norm_gain,
    w_filter_b,
    w_filter_c,
    w_filter_v,
    filter_taps,
    w_query,
    retention_gate_matrix,
    w_input,
    forget_gap,
    additive_fade_log,
    head_gain,
    initial_state,
    w_out_filter,
    w_out_rec,
):
    gathered = lax.all_gather(tokens, "tp", axis=0, tiled=True)
    widened = gathered.astype(jnp.float32)
    normed = (
        widened
        * lax.rsqrt(jnp.mean(widened * widened, axis=-1, keepdims=True) + epsilon)
        * norm_gain
    ).astype(jnp.bfloat16)
    recur_cols = (
        lax.all_gather(w_query, "sp", axis=0, tiled=True),
        lax.all_gather(retention_gate_matrix, "sp", axis=0, tiled=True),
        lax.all_gather(w_input, "sp", axis=0, tiled=True),
    )
    within_block, scaled_query, decay_total, end_state = local_recurrence(
        normed, recur_cols, forget_gap, additive_fade_log
    )
    filter_cols = (
        lax.all_gather(w_filter_b, "sp", axis=0, tiled=True),
        lax.all_gather(w_filter_c, "sp", axis=0, tiled=True),
        lax.all_gather(w_filter_v, "sp", axis=0, tiled=True),
    )
    gate_out = project(normed, filter_cols[0])
    product = project(normed, filter_cols[1]).astype(jnp.float32) * project(
        normed, filter_cols[2]
    ).astype(jnp.float32)
    length = product.shape[0]
    last_rows = product[length - (TAPS - 1) :]
    before = shifted(last_rows, "sp", 1)
    decay_before, state_before = prefix(
        (decay_total, end_state),
        "sp",
        chain_combine,
        (jnp.zeros_like(decay_total), jnp.zeros_like(end_state)),
    )
    incoming_state = jnp.exp(decay_before)[:, :, None] * initial_state + state_before
    unmixed_output = within_block + jnp.einsum(
        "oql,qlz->oqz", scaled_query, incoming_state, precision=highest_precision
    )
    rec_out = (
        (
            unmixed_output
            * lax.rsqrt(jnp.mean(unmixed_output * unmixed_output, axis=-1, keepdims=True) + epsilon)
            * head_gain
        )
        .astype(jnp.bfloat16)
        .reshape(length, -1)
    )
    padded = jnp.concatenate([before, product], axis=0)
    filtered = jnp.zeros_like(product)
    for offset in range(TAPS):
        filtered = filtered + filter_taps[offset] * padded[offset : offset + length]
    filter_out = (gate_out.astype(jnp.float32) * filtered).astype(jnp.bfloat16)
    return lax.psum_scatter(
        (
            jnp.dot(filter_out, w_out_filter, preferred_element_type=jnp.float32)
            + jnp.dot(rec_out, w_out_rec, preferred_element_type=jnp.float32)
        ).astype(jnp.bfloat16),
        "tp",
        scatter_dimension=0,
        tiled=True,
    )


def solution(mesh):
    placed = (
        P(("sp", "tp"), None),
        P(),
        P("sp", "tp"),
        P("sp", "tp"),
        P("sp", "tp"),
        P(None, "tp"),
        P("sp", "tp"),
        P("sp", "tp"),
        P("sp", "tp"),
        P("tp"),
        P("sp", "tp"),
        P(),
        P("tp", None, None),
        P("tp", None),
        P("tp", None),
    )
    return jax.shard_map(
        body, mesh=mesh, in_specs=placed, out_specs=P(("sp", "tp"), None), check_vma=False
    )
```

profile of v0, /device:TPU:17, one launch (start us, length us, event | category | flops | bytes accessed | tf_op | source)
XLA Modules:
  0.0 289.2 jit_solution(7823043393639604807)
XLA Ops:
  6.5 0.7 all-gather.14.cloned.1.call-update
  7.3 0.7 all-gather.18.cloned.1.call-update
  8.1 0.7 all-gather.16.cloned.1.call-update
  10.6 7.7 %all_gather.31 = bf16[128,2048]{1,0:T(8,128)(2,1)S(1)} all-gather(bf16[32,2048]{1,0:T(8,128)(2,1)S(1)} %copy-done.1), channel_id=1, replica_groups=mesh['sp'=8,'tp'=4] {'tp'}, dimensions={0}, use_global_device_ids=true | all-gather | bytes 655360 | tf_op jit(solution)/shard_map/all_gather | solution.py:120
  19.0 29.4 %all-gather.14.cloned.1.call-done = bf16[2048,256]{1,0:T(8,128)(2,1)} async-done(((bf16[256,256]{1,0:T(8,128)(2,1)}), bf16[2048,256]{1,0:T(8,128)(2,1)}) %all-gather.14.cloned.1.call-update) | async-done | bytes 1048592 | tf_op jit(solution)/shard_map/all_gather | solution.py:129
  48.4 1.6 log-plus-one_add_fusion
  50.3 39.3 %all-gather.18.cloned.1.call-done = bf16[2048,256]{1,0:T(8,128)(2,1)} async-done(((bf16[256,256]{1,0:T(8,128)(2,1)}), bf16[2048,256]{1,0:T(8,128)(2,1)}) %all-gather.18.cloned.1.call-update) | async-done | bytes 1048592 | tf_op jit(solution)/shard_map/all_gather | solution.py:128
  89.5 1.6 fusion.18
  91.2 39.5 %all-gather.16.cloned.1.call-done = bf16[2048,256]{1,0:T(8,128)(2,1)} async-done(((bf16[256,256]{1,0:T(8,128)(2,1)}), bf16[2048,256]{1,0:T(8,128)(2,1)}) %all-gather.16.cloned.1.call-update) | async-done | bytes 1048592 | tf_op jit(solution)/shard_map/all_gather | solution.py:130
  130.7 1.6 divide_multiply_fusion
  132.4 2.7 while.26
  135.1 23.0 %all-gather = bf16[16,128,128]{2,1,0:T(8,128)(2,1)S(1)} all-gather(bf16[2,128,128]{2,1,0:T(8,128)(2,1)S(1)} %convert_element_type.87), channel_id=2, replica_groups=mesh['sp'=8,'tp'=4] {'sp'}, dimensions={0}, use_global_device_ids=true | all-gather | bytes 589824 | tf_op jit(solution)/shard_map/all_gather | solution.py:24
  158.3 13.8 %all_gather.38 = bf16[8,2,128]{2,1,0:T(2,128)(2,1)S(1)} all-gather(bf16[1,2,128]{2,1,0:T(2,128)(2,1)S(1)} %slice.60), channel_id=1, replica_groups=mesh['sp'=8,'tp'=4] {'sp'}, dimensions={0}, use_global_device_ids=true | all-gather | bytes 4608 | tf_op jit(solution)/shard_map/all_gather | solution.py:24
  172.1 0.7 while.25
  173.3 1.6 fusion.27
  174.9 39.2 %all-gather.12.cloned.1.call-done = bf16[2048,256]{1,0:T(8,128)(2,1)} async-done(((bf16[256,256]{1,0:T(8,128)(2,1)}), bf16[2048,256]{1,0:T(8,128)(2,1)}) %all-gather.12.cloned.1.call-update) | async-done | bytes 1048592 | tf_op jit(solution)/shard_map/all_gather | solution.py:138
  214.1 1.6 fusion.26
  215.7 2.2 collective-permute-start
  217.9 0.9 copy-done.2
  219.3 0.7 copy-done.5
  220.0 35.1 %all-gather.8.cloned.1.call-done = bf16[2048,256]{1,0:T(8,128)(2,1)} async-done(((bf16[256,256]{1,0:T(8,128)(2,1)}), bf16[2048,256]{1,0:T(8,128)(2,1)}) %all-gather.8.cloned.1.call-update) | async-done | bytes 1048592 | tf_op jit(solution)/shard_map/all_gather | solution.py:136
  255.1 2.0 fusion.42
  257.1 2.4 fusion.16
  259.5 22.8 %reduce-scatter.2.cloned.1.call-done = bf16[32,2048]{1,0:T(8,128)(2,1)} async-done(((bf16[128,2048]{1,0:T(8,128)(2,1)}), bf16[32,2048]{1,0:T(8,128)(2,1)}) %reduce-scatter.2.cloned.1.call-update) | async-done | bytes 131088 | tf_op jit(solution)/shard_map/reduce_scatter | solution.py:171
  (78 shorter events, 7.2 us)
Async XLA Ops:
  6.5 248.6 %copy-start = (bf16[256,2048]{1,0:T(8,128)(2,1)S(1)}, bf16[256,2048]{1,0:T(8,128)(2,1)}, u32[]{:S(2)}) copy-start(bf16[256,2048]{1,0:T(8,128)(2,1)} %param.32) | copy-start | bytes 3145732
  6.5 41.9 %all-gather.14.cloned.1.call-start = ((), (), s32[]{:S(2)}) async-start(), calls=%async_computation.4 | async-start | bytes 1179648 | tf_op jit(solution)/shard_map/all_gather | solution.py:129
  7.3 82.3 %all-gather.18.cloned.1.call-start = ((), (), s32[]{:S(2)}) async-start(), calls=%async_computation.6 | async-start | bytes 1179648 | tf_op jit(solution)/shard_map/all_gather | solution.py:128
  8.0 122.7 %all-gather.16.cloned.1.call-start = ((), (), s32[]{:S(2)}) async-start(), calls=%async_computation.5 | async-start | bytes 1179648 | tf_op jit(solution)/shard_map/all_gather | solution.py:130
  8.7 164.6 %all-gather.10.cloned.1.call-start = ((), (), s32[]{:S(2)}) async-start(), calls=%async_computation.2 | async-start | bytes 1179648 | tf_op jit(solution)/shard_map/all_gather | solution.py:137
  9.3 1.2 copy-start.1
  9.3 204.7 %all-gather.12.cloned.1.call-start = ((), (), s32[]{:S(2)}) async-start(), calls=%async_computation.3 | async-start | bytes 1179648 | tf_op jit(solution)/shard_map/all_gather | solution.py:138
  9.9 245.2 %all-gather.8.cloned.1.call-start = ((), (), s32[]{:S(2)}) async-start(), calls=%async_computation.1 | async-start | bytes 1179648 | tf_op jit(solution)/shard_map/all_gather | solution.py:136
  10.5 271.8 %reduce-scatter.2.cloned.1.call-start = ((), (), s32[]{:S(2)}) async-start(), calls=%async_computation.7 | async-start | bytes 655360 | tf_op jit(solution)/shard_map/reduce_scatter | solution.py:171
  18.3 0.7 copy-start.4
  18.3 30.1 %copy-start.6 = (f32[128,256]{1,0:T(8,128)S(1)}, f32[128,256]{1,0:T(8,128)}, u32[]{:S(2)}) copy-start(f32[128,256]{1,0:T(8,128)} %param.29) | copy-start | bytes 393220
  18.4 29.9 %copy-start.3 = (f32[2048]{0:T(1024)S(1)}, f32[2048]{0:T(1024)}, u32[]{:S(2)}) copy-start(f32[2048]{0:T(1024)} %param.20) | copy-start | bytes 24580
  18.9 29.5 %copy-start.7 = (f32[256]{0:T(256)S(1)}, f32[256]{0:T(256)}, u32[]{:S(2)}) copy-start(f32[256]{0:T(256)} %param.28) | copy-start | bytes 3076
  215.7 39.4 %collective-permute-start = (f32[2,256]{1,0:T(2,128)S(1)}, f32[2,256]{1,0:T(2,128)S(1)}, u32[]{:S(2)}, u32[]{:S(2)}) collective-permute-start(f32[2,256]{1,0:T(2,128)S(1)} %slice.34), channel_id=1, source_target_pairs={{0,4},{4,8},{8,12},{12,16},{16,20},{20,24},{24,28},{1,5},{5,9},{9,... | collective-permute-start | bytes 6152 | tf_op jit(solution)/shard_map/ppermute | solution.py:18
  217.8 0.9 copy-start.2
  219.2 0.7 copy-start.5
Sparse Core Ops, SparseCore 0:
  9.5 38.8 all-gather.13
  50.5 38.9 all-gather.17
  91.7 38.9 all-gather.15
  132.7 40.5 all-gather.9
  175.3 38.7 all-gather.11
  216.1 38.9 all-gather.7
  259.6 22.6 reduce-scatter.1
where the time goes:
time: 291 us; the launch traced here: 289 us
  waiting for transfers between devices  209 us (72%)
  blocking collectives  44.5 us (15%)
  matrix products  15 us (5%)
  between operations  13.7 us (5%)
    all_gather x1, waiting for transfers between devices, body(): lax.all_gather(w_input, 'sp', axis=0, tiled=True)  39.5 us
    all_gather x1, waiting for transfers between devices, body(): lax.all_gather(w_query, 'sp', axis=0, tiled=True)  39.3 us
    all_gather x1, waiting for transfers between devices, body(): lax.all_gather(w_filter_v, 'sp', axis=0, tiled=True)  39.2 us
    all_gather x2, blocking collectives, prefix(): lax.all_gather(a.astype(kind), axis)  36.8 us
    all_gather x1, waiting for transfers between devices, body(): lax.all_gather(w_filter_b, 'sp', axis=0, tiled=True)  35.1 us
    all_gather x1, waiting for transfers between devices, body(): lax.all_gather(retention_gate_matrix, 'sp', axis=0, tiled=True)  29.4 us
    reduce_scatter x1, waiting for transfers between devices, body(): lax.psum_scatter((jnp.dot(filter_out, w_out_filter, preferred_element_typ...  22.8 us
    dot_general x5, matrix products, project(): jnp.dot(normed, weight, preferred_element_type=jnp.float32)  7.94 us
  transfers between devices with their start and end apart: 8, of which 7 were waited for; matrix products, arithmetic and copies ran while one was open for 4% of the time, Pallas kernels for 0%

commit v1 on v0

v1 whole, which is shorter than its diff:
```python
import functools

import jax
import jax.numpy as jnp
from jax import lax
from jax.experimental import pallas as pl
from jax.experimental.pallas import tpu as pltpu
from jax.sharding import PartitionSpec as P

HEAD_DIM = 128
TAPS = 3
SHARES = 4
CHUNKS = 4
PROJ = 6
EPS = 1e-06
MESH = pl.DeviceIdType.MESH
F32 = jnp.float32
BF16 = jnp.bfloat16


def repeat(count, step):
    if count <= 4:
        for i in range(count):
            step(i)
    else:
        lax.fori_loop(0, count, lambda i, c: (step(i), c)[1], 0)


def dot(a, b):
    return jnp.dot(a, b, preferred_element_type=F32)


def dot_on(a, b, da, db):
    return lax.dot_general(a, b, (((da,), (db,)), ((), ())), preferred_element_type=F32)


def mix_kernel(
    n_sp,
    n_tp,
    tok,
    gain,
    taps,
    gap,
    fade,
    hgain,
    init,
    wq,
    wf,
    wi,
    wc,
    wv,
    wb,
    wof,
    wor,
    out,
    xs,
    xbuf,
    wbuf,
    own,
    psend,
    pland,
    sland,
    gland,
    sin,
    pad,
    obuf,
    oland,
    vof,
    vor,
    tok_s,
    tok_r,
    w_l,
    w_s,
    w_r,
    p_s,
    p_r,
    s_s,
    s_r,
    g_s,
    g_r,
    h_s,
    h_r,
    o_s,
    o_r,
    v_l,
):
    sp, tp = lax.axis_index("sp"), lax.axis_index("tp")
    group = n_sp // SHARES
    z, r = lax.div(sp, group), lax.rem(sp, group)
    t_loc = tok.shape[0]
    length = t_loc * n_tp
    rows, width = wq.shape
    depth = rows * group
    heads = width // HEAD_DIM
    weights = (wq, wf, wi, wc, wv, wb)

    def shift_z(by):
        return lax.rem(z + by + SHARES, SHARES)

    def shift_t(by):
        return lax.rem(tp + by + n_tp, n_tp)

    def shift_r(by):
        return lax.rem(r + by + group, group)

    def send(src, dst, ss, rs, to):
        return pltpu.make_async_remote_copy(
            src_ref=src, dst_ref=dst, send_sem=ss, recv_sem=rs, device_id=to, device_id_type=MESH
        )

    barrier = pltpu.get_barrier_semaphore()

    def hail(a, b):
        pl.semaphore_signal(barrier, inc=1, device_id=(a, b), device_id_type=MESH)

    repeat(group - 1, lambda i: hail(z * group + shift_r(i + 1), tp))
    spread = [(a, b) for a in range(SHARES) for b in range(n_tp) if (a, b) != (0, 0)]
    for a, b in spread:
        hail(shift_z(a) * group + r, shift_t(b))
    after, before = lax.rem(sp + 1, n_sp), lax.rem(sp + n_sp - 1, n_sp)
    hail(after, tp)
    hail(before, tp)

    mine = pl.ds(pl.multiple_of(r * rows, rows), rows)
    for p in range(PROJ):
        pltpu.make_async_copy(weights[p], wbuf.at[p, mine], w_l.at[p]).start()
    pltpu.make_async_copy(wof, vof, v_l.at[0]).start()
    pltpu.make_async_copy(wor, vor, v_l.at[1]).start()

    x = tok[...].astype(F32)
    normed = x * lax.rsqrt(jnp.mean(x * x, axis=-1, keepdims=True) + EPS) * gain[...]
    normed = normed.astype(BF16)
    for a in range(SHARES):
        xs[a] = normed[:, a * depth : (a + 1) * depth]
    xbuf[z, tp] = xs[z]

    pl.semaphore_wait(barrier, group - 1 + len(spread) + 2)

    def token_copy(a, b):
        to = (shift_z(a) * group + r, shift_t(b))
        return send(xs.at[shift_z(a)], xbuf.at[z, tp], tok_s.at[a, b], tok_r.at[a, b], to)

    def token_landing(a, b):
        to = (shift_z(-a) * group + r, shift_t(-b))
        return send(
            xs.at[0], xbuf.at[shift_z(-a), shift_t(-b)], tok_s.at[a, b], tok_r.at[a, b], to
        )

    def weight_copy(p, i):
        to = (z * group + shift_r(i + 1), tp)
        return send(weights[p], wbuf.at[p, mine], w_s.at[p, i], w_r.at[p, i], to)

    def weight_landing(p, i):
        src = shift_r(-i - 1)
        theirs = pl.ds(pl.multiple_of(src * rows, rows), rows)
        return send(
            weights[p], wbuf.at[p, theirs], w_s.at[p, i], w_r.at[p, i], (z * group + src, tp)
        )

    repeat(group - 1, lambda i: weight_copy(0, i).start())
    for a, b in spread:
        token_copy(a, b).start()
    for p in range(1, PROJ):
        repeat(group - 1, lambda i: weight_copy(p, i).start())

    for a, b in spread:
        token_landing(a, b).wait_recv()

    def part_copy(p, a):
        to = (shift_z(a) * group + r, tp)
        return send(psend.at[p, shift_z(a)], pland.at[p, a], p_s.at[p, a], p_r.at[p, a], to)

    def project(p):
        pltpu.make_async_copy(weights[p], wbuf.at[p, mine], w_l.at[p]).wait()
        repeat(group - 1, lambda i: weight_landing(p, i).wait_recv())
        full = xbuf[...].reshape(SHARES * length, depth)
        part = dot(full, wbuf[p]).reshape(SHARES, length, width)
        own[p] = part
        psend[p] = part.astype(BF16)
        for a in (2, 1, 3):
            part_copy(p, a).start()

    def total(p):
        for a in range(1, SHARES):
            part_copy(p, a).wait_recv()
        s = own[p, z]
        for a in range(1, SHARES):
            s = s + pland[p, a].astype(F32)
        return s.astype(BF16).astype(F32)

    for p in range(4):
        project(p)

    query, logit, value = total(0), total(1), total(2)
    rate = gap[...] / (1.0 + jnp.exp(logit))
    decay = jnp.log1p(-rate) + fade[...]
    value = (value / (1.0 + jnp.exp(-value))).astype(BF16)
    below = lax.broadcasted_iota(jnp.int32, (length, length), 0) >= lax.broadcasted_iota(
        jnp.int32, (length, length), 1
    )
    running = jnp.dot(
        below.astype(F32), decay, preferred_element_type=F32, precision=lax.Precision.HIGHEST
    )
    middle = running[length // 2 - 1 : length // 2]
    last = running[length - 1 : length]
    query_mid = (query * jnp.exp(running - middle)).astype(BF16)
    key_mid = (rate * jnp.exp(middle - running)).astype(BF16)
    key_end = (rate * jnp.exp(last - running)).astype(BF16)
    query_in = (query * jnp.exp(running)).astype(BF16)
    within = []
    cuts = [slice(h * HEAD_DIM, (h + 1) * HEAD_DIM) for h in range(heads)]
    for cut in cuts:
        sland[r, 0:HEAD_DIM, cut] = dot_on(value[:, cut], key_end[:, cut], 0, 0).astype(BF16)
    coarse = last.astype(BF16).astype(F32)
    upper = lax.broadcasted_iota(jnp.int32, (16, width), 0) < 8
    sland[r, HEAD_DIM : HEAD_DIM + 16, :] = jnp.where(upper, coarse, last - coarse).astype(BF16)

    def state_copy(i):
        to = (z * group + shift_r(i + 1), tp)
        return send(sland.at[r], sland.at[r], s_s.at[i], s_r.at[i], to)

    def state_landing(i):
        src = shift_r(-i - 1)
        return send(sland.at[src], sland.at[src], s_s.at[i], s_r.at[i], (z * group + src, tp))

    repeat(group - 1, lambda i: state_copy(i).start())
    for cut in cuts:
        scores = dot_on(query_mid[:, cut], key_mid[:, cut], 1, 1)
        scores = jnp.where(below, scores, 0.0).astype(BF16)
        within.append(dot(scores, value[:, cut]))

    for p in range(4, PROJ):
        project(p)

    repeat(group - 1, lambda i: state_landing(i).wait_recv())

    def parts_of(ref, i):
        tail = ref[i, HEAD_DIM : HEAD_DIM + 16, :].astype(F32)
        return ref[i, 0:HEAD_DIM, :].astype(F32), tail[0:1] + tail[8:9]

    def join(i, carry):
        whole, whole_decay, near, near_decay = carry
        state, fall = parts_of(sland, i)
        factor = jnp.exp(fall)
        whole, whole_decay = factor * whole + state, whole_decay + fall
        earlier = i < r
        near = jnp.where(earlier, factor * near + state, near)
        near_decay = jnp.where(earlier, near_decay + fall, near_decay)
        return whole, whole_decay, near, near_decay

    blank = jnp.zeros((HEAD_DIM, width), F32)
    line = jnp.zeros((1, width), F32)
    carry = (blank, line, blank, line)
    if group <= 4:
        for i in range(group):
            carry = join(i, carry)
    else:
        carry = lax.fori_loop(0, group, join, carry)
    whole, whole_decay, near, near_decay = carry
    gland[z, 0:HEAD_DIM, :] = whole.astype(BF16)
    coarse = whole_decay.astype(BF16).astype(F32)
    gland[z, HEAD_DIM : HEAD_DIM + 16, :] = jnp.where(upper, coarse, whole_decay - coarse).astype(
        BF16
    )

    def group_copy(a):
        return send(
            gland.at[z], gland.at[z], g_s.at[a], g_r.at[a], (shift_z(a) * group + r, tp)
        )

    def group_landing(a):
        src = shift_z(-a)
        return send(gland.at[src], gland.at[src], g_s.at[a], g_r.at[a], (src * group + r, tp))

    for a in range(1, SHARES):

        @pl.when(z + a < SHARES)
        def _():
            group_copy(a).start()

    gate_in, filter_value = total(3), total(4)
    product = gate_in * filter_value
    pad[8 : 8 + length] = product

    halo = send(pad.at[pl.ds(length, 8)], pad.at[pl.ds(0, 8)], h_s, h_r, (after, tp))
    halo.start()
    gate_out = total(5)
    halo.wait_recv()
    edge = jnp.where(sp > 0, pad[0:8], 0.0)
    halo.wait_send()
    pad[0:8] = edge
    filtered = taps[TAPS - 1 : TAPS] * product
    for j in range(TAPS - 1):
        start = 8 - (TAPS - 1) + j
        filtered = filtered + taps[j : j + 1] * pad[start : start + length]
    filter_out = (gate_out * filtered).astype(BF16)

    for h in range(heads):
        sin[:, cuts[h]] = init[h].T
    for a in range(1, SHARES):

        @pl.when(z >= a)
        def _():
            group_landing(a).wait_recv()

    for i in range(SHARES - 1):

        @pl.when(i < z)
        def _():
            state, fall = parts_of(gland, i)
            sin[...] = jnp.exp(fall) * sin[...] + state

    incoming = (jnp.exp(near_decay) * sin[...] + near).astype(BF16)
    rec = []
    for h in range(heads):
        raw = within[h] + dot_on(query_in[:, cuts[h]], incoming[:, cuts[h]], 1, 1)
        scale = lax.rsqrt(jnp.mean(raw * raw, axis=-1, keepdims=True) + EPS)
        rec.append((raw * scale * hgain[...]).astype(BF16))
    rec_out = jnp.concatenate(rec, axis=-1)

    pltpu.make_async_copy(wof, vof, v_l.at[0]).wait()
    pltpu.make_async_copy(wor, vor, v_l.at[1]).wait()
    d_out = wof.shape[1]
    cols = d_out // CHUNKS

    def out_copy(c, b):
        to = (sp, shift_t(b))
        return send(obuf.at[c, shift_t(b)], oland.at[c, b], o_s.at[c, b], o_r.at[c, b], to)

    for c in range(CHUNKS):
        cut = slice(c * cols, (c + 1) * cols)
        part = dot(filter_out, vof[:, cut]) + dot(rec_out, vor[:, cut])
        obuf[c] = part.astype(BF16).reshape(n_tp, t_loc, cols)
        for b in range(1, n_tp):
            out_copy(c, b).start()
    for c in range(CHUNKS):
        s = obuf[c, tp].astype(F32)
        for b in range(1, n_tp):
            out_copy(c, b).wait_recv()
            s = s + oland[c, b].astype(F32)
        out[:, c * cols : (c + 1) * cols] = s.astype(BF16)

    for a, b in spread:
        token_copy(a, b).wait_send()
    for p in range(PROJ):
        repeat(group - 1, lambda i: weight_copy(p, i).wait_send())
        for a in range(1, SHARES):
            part_copy(p, a).wait_send()
    repeat(group - 1, lambda i: state_copy(i).wait_send())
    for a in range(1, SHARES):

        @pl.when(z + a < SHARES)
        def _():
            group_copy(a).wait_send()

    for c in range(CHUNKS):
        for b in range(1, n_tp):
            out_copy(c, b).wait_send()


def body(
    tokens,
    norm_gain,
    w_filter_b,
    w_filter_c,
    w_filter_v,
    filter_taps,
    w_query,
    retention_gate_matrix,
    w_input,
    forget_gap,
    additive_fade_log,
    head_gain,
    initial_state,
    w_out_filter,
    w_out_rec,
):
    n_sp, n_tp = lax.axis_size("sp"), lax.axis_size("tp")
    group = n_sp // SHARES
    t_loc, d = tokens.shape
    rows, width = w_query.shape
    depth = rows * group
    length = t_loc * n_tp
    d_out = w_out_filter.shape[1]
    cols = d_out // CHUNKS
    vmem = pl.BlockSpec(memory_space=pltpu.VMEM)
    hbm = pl.BlockSpec(memory_space=pl.ANY)
    peers = max(group - 1, 1)
    dma = pltpu.SemaphoreType.DMA
    return pl.pallas_call(
        functools.partial(mix_kernel, n_sp, n_tp),
        out_shape=jax.ShapeDtypeStruct((t_loc, d_out), BF16),
        in_specs=[vmem] * 7 + [hbm] * 8,
        out_specs=vmem,
        scratch_shapes=[
            pltpu.VMEM((SHARES, t_loc, depth), BF16),
            pltpu.VMEM((SHARES, n_tp, t_loc, depth), BF16),
            pltpu.VMEM((PROJ, depth, width), BF16),
            pltpu.VMEM((PROJ, SHARES, length, width), F32),
            pltpu.VMEM((PROJ, SHARES, length, width), BF16),
            pltpu.VMEM((PROJ, SHARES, length, width), BF16),
            pltpu.VMEM((group, HEAD_DIM + 16, width), BF16),
            pltpu.VMEM((SHARES, HEAD_DIM + 16, width), BF16),
            pltpu.VMEM((HEAD_DIM, width), F32),
            pltpu.VMEM((length + 8, width), F32),
            pltpu.VMEM((CHUNKS, n_tp, t_loc, cols), BF16),
            pltpu.VMEM((CHUNKS, n_tp, t_loc, cols), BF16),
            pltpu.VMEM(w_out_filter.shape, BF16),
            pltpu.VMEM(w_out_rec.shape, BF16),
            dma((SHARES, n_tp)),
            dma((SHARES, n_tp)),
            dma((PROJ,)),
            dma((PROJ, peers)),
            dma((PROJ, peers)),
            dma((PROJ, SHARES)),
            dma((PROJ, SHARES)),
            dma((peers,)),
            dma((peers,)),
            dma((SHARES,)),
            dma((SHARES,)),
            dma,
            dma,
            dma((CHUNKS, n_tp)),
            dma((CHUNKS, n_tp)),
            dma((2,)),
        ],
        compiler_params=pltpu.CompilerParams(
            collective_id=0, has_side_effects=True, vmem_limit_bytes=60 * 1024 * 1024
        ),
    )(
        tokens,
        norm_gain.reshape(1, d),
        filter_taps,
        forget_gap.reshape(1, width),
        additive_fade_log,
        head_gain.reshape(1, HEAD_DIM),
        initial_state,
        w_query,
        retention_gate_matrix,
        w_input,
        w_filter_c,
        w_filter_v,
        w_filter_b,
        w_out_filter,
        w_out_rec,
    )


def solution(mesh):
    placed = (
        P(("sp", "tp"), None),
        P(),
        P("sp", "tp"),
        P("sp", "tp"),
        P("sp", "tp"),
        P(None, "tp"),
        P("sp", "tp"),
        P("sp", "tp"),
        P("sp", "tp"),
        P("tp"),
        P("sp", "tp"),
        P(),
        P("tp", None, None),
        P("tp", None),
        P("tp", None),
    )
    return jax.shard_map(
        body, mesh=mesh, in_specs=placed, out_specs=P(("sp", "tp"), None), check_vma=False
    )
```

time: 291 us -> 70.9 us (0.24)
  waiting for transfers between devices: 209 us -> 0 us
  Pallas kernels: 0 us -> 69.2 us
  blocking collectives: 44.5 us -> 0 us
  matrix products: 15 us -> 0 us
  between operations: 13.7 us -> 0.01 us
    all_gather x6 -> x0, waiting for transfers between devices: 183 us -> none  [the longest x1 39.5 us: body(): lax.all_gather(w_input, 'sp', axis=0, tiled=True)]
    pallas_call x0 -> x1, Pallas kernels: none -> 69.2 us  [body(): pl.pallas_call(functools.partial(mix_kernel, n_sp, n_tp), out_shape=jax.S...]
    all_gather x3 -> x0, blocking collectives: 44.5 us -> none  [the longest x2 36.8 us: prefix(): lax.all_gather(a.astype(kind), axis)]
    reduce_scatter x1 -> x0, waiting for transfers between devices: 22.8 us -> none  [body(): lax.psum_scatter((jnp.dot(filter_out, w_out_filter, preferred_element_typ...]
    dot_general x16 -> x0, matrix products: 15 us -> none  [the longest x5 7.94 us: project(): jnp.dot(normed, weight, preferred_element_type=jnp.float32)]
    unnamed x7 -> x0, waiting for transfers between devices: 3.68 us -> none
  transfers between devices with their start and end apart: 8 -> 0, of which waited for: 7 -> 0; matrix products, arithmetic and copies ran while one was open for 4% -> 0% of each run, Pallas kernels for 0% -> 0%
where the time goes in v1:
time: 70.9 us; the launch traced here: 70.8 us
  Pallas kernels  69.2 us (98%)
  local copies, waits for them, and re-layouts  1.57 us (2%)
    pallas_call x1, Pallas kernels, body(): pl.pallas_call(functools.partial(mix_kernel, n_sp, n_tp), out_shape=jax.S...  69.2 us
    unnamed x1, local copies, waits for them, and re-layouts  1.57 us

profile of v1, /device:TPU:17, one launch (start us, length us, event | category | flops | bytes accessed | tf_op | source)
XLA Modules:
  0.0 70.8 jit_solution(7973026062041420489)
XLA Ops:
  0.0 69.2 %shard_map.145 = bf16[32,2048]{1,0:T(8,128)(2,1)} custom-call(bf16[32,2048]{1,0:T(8,128)(2,1)} %tok.1, f32[1,2048]{1,0:T(1,128)} %bitcast.3, f32[3,256]{1,0:T(4,128)} %taps.1, f32[1,256]{1,0:T(1,128)} %bitcast.4, f32[128,256]{1,0:T(8,128)} %fade.1, f32[1,128]{1,0:T(1,128)} %bitcast.5, f32[2,128,128]{2,1,0:T(8,128)} %init.1, bf16[256,256]{1,0:T(8,128)(2,1)} %wq.1, ...), custom_call_target="tpu_custom_call" | custom-call | tf_op jit(solution)/shard_map/pallas_call | solution.py:390
  69.2 1.6 %copy.17 = bf16[32,2048]{1,0:T(8,128)(2,1)} copy(bf16[32,2048]{1,0:T(8,128)(2,1)} %shard_map.145) | data formatting | bytes 262144

commit v2 on v1

--- a/solution.py
+++ b/solution.py
@@ -65,6 +65,8 @@
     pad,
     obuf,
     oland,
+    osend,
+    acc,
     vof,
     vor,
     tok_s,
@@ -97,8 +99,11 @@
     def shift_z(by):
         return lax.rem(z + by + SHARES, SHARES)
 
-    def shift_t(by):
-        return lax.rem(tp + by + n_tp, n_tp)
+    t_half, t_side = lax.div(tp, 2), lax.rem(tp, 2)
+    mate = 2 * t_half + 1 - t_side
+    across = 2 * (1 - t_half) + t_side
+    corner = 2 * (1 - t_half) + 1 - t_side
+    on_tp = (tp, mate, across, corner)
 
     def shift_r(by):
         return lax.rem(r + by + group, group)
@@ -116,7 +121,7 @@
     repeat(group - 1, lambda i: hail(z * group + shift_r(i + 1), tp))
     spread = [(a, b) for a in range(SHARES) for b in range(n_tp) if (a, b) != (0, 0)]
     for a, b in spread:
-        hail(shift_z(a) * group + r, shift_t(b))
+        hail(shift_z(a) * group + r, on_tp[b])
     after, before = lax.rem(sp + 1, n_sp), lax.rem(sp + n_sp - 1, n_sp)
     hail(after, tp)
     hail(before, tp)
@@ -137,14 +142,20 @@
     pl.semaphore_wait(barrier, group - 1 + len(spread) + 2)
 
     def token_copy(a, b):
-        to = (shift_z(a) * group + r, shift_t(b))
-        return send(xs.at[shift_z(a)], xbuf.at[z, tp], tok_s.at[a, b], tok_r.at[a, b], to)
+        if b == 0:
+            to = (shift_z(a) * group + r, tp)
+            return send(xs.at[shift_z(a)], xbuf.at[z, tp], tok_s.at[a, b], tok_r.at[a, b], to)
+        piece = xbuf.at[shift_z(-a), across if b == 3 else tp]
+        to = across if b == 2 else mate
+        return send(piece, piece, tok_s.at[a, b], tok_r.at[a, b], (sp, to))
 
     def token_landing(a, b):
-        to = (shift_z(-a) * group + r, shift_t(-b))
-        return send(
-            xs.at[0], xbuf.at[shift_z(-a), shift_t(-b)], tok_s.at[a, b], tok_r.at[a, b], to
-        )
+        piece = xbuf.at[shift_z(-a), on_tp[b]]
+        if b == 0:
+            to = (shift_z(-a) * group + r, tp)
+            return send(xs.at[0], piece, tok_s.at[a, b], tok_r.at[a, b], to)
+        frm = across if b == 2 else mate
+        return send(piece, piece, tok_s.at[a, b], tok_r.at[a, b], (sp, frm))
 
     def weight_copy(p, i):
         to = (z * group + shift_r(i + 1), tp)
@@ -157,39 +168,56 @@
             weights[p], wbuf.at[p, theirs], w_s.at[p, i], w_r.at[p, i], (z * group + src, tp)
         )
 
-    repeat(group - 1, lambda i: weight_copy(0, i).start())
-    for a, b in spread:
-        token_copy(a, b).start()
-    for p in range(1, PROJ):
+    for a in (2, 1, 3):
+        token_copy(a, 0).start()
+    for b in (2, 1):
+        token_copy(0, b).start()
+    for p in range(PROJ):
         repeat(group - 1, lambda i: weight_copy(p, i).start())
-
-    for a, b in spread:
-        token_landing(a, b).wait_recv()
-
-    def part_copy(p, a):
-        to = (shift_z(a) * group + r, tp)
-        return send(psend.at[p, shift_z(a)], pland.at[p, a], p_s.at[p, a], p_r.at[p, a], to)
+    for a in (1, 3, 2):
+        token_landing(a, 0).wait_recv()
+        for b in (2, 1):
+            token_copy(a, b).start()
+    for a in (0, 1, 3, 2):
+        token_landing(a, 2).wait_recv()
+        token_copy(a, 3).start()
+    for a in (0, 1, 3, 2):
+        for b in (1, 3):
+            token_landing(a, b).wait_recv()
+
+    half, side = lax.div(z, 2), lax.rem(z, 2)
+    near_z = 2 * half + 1 - side
+    far_z = 2 * (1 - half) + side
+
+    def part_copy(p, k):
+        to = ((near_z if k < 2 else far_z) * group + r, tp)
+        return send(psend.at[p, k], pland.at[p, k], p_s.at[p, k], p_r.at[p, k], to)
 
     def project(p):
         pltpu.make_async_copy(weights[p], wbuf.at[p, mine], w_l.at[p]).wait()
         repeat(group - 1, lambda i: weight_landing(p, i).wait_recv())
         full = xbuf[...].reshape(SHARES * length, depth)
-        part = dot(full, wbuf[p]).reshape(SHARES, length, width)
-        own[p] = part
-        psend[p] = part.astype(BF16)
-        for a in (2, 1, 3):
-            part_copy(p, a).start()
+        own[p] = dot(full, wbuf[p]).reshape(SHARES, length, width)
+        psend[p, 0] = own[p, 2 * (1 - half) + 1 - side].astype(BF16)
+        part_copy(p, 0).start()
+        psend[p, 1] = own[p, near_z].astype(BF16)
+        part_copy(p, 1).start()
+
+    def relay(p):
+        part_copy(p, 0).wait_recv()
+        psend[p, 2] = (own[p, far_z] + pland[p, 0].astype(F32)).astype(BF16)
+        part_copy(p, 2).start()
 
     def total(p):
-        for a in range(1, SHARES):
-            part_copy(p, a).wait_recv()
-        s = own[p, z]
-        for a in range(1, SHARES):
-            s = s + pland[p, a].astype(F32)
+        part_copy(p, 1).wait_recv()
+        part_copy(p, 2).wait_recv()
+        s = own[p, z] + pland[p, 1].astype(F32) + pland[p, 2].astype(F32)
         return s.astype(BF16).astype(F32)
 
-    for p in range(4):
+    for p in range(PROJ):
         project(p)
+        if 0 < p < PROJ - 1:
+            relay(p - 1)
 
     query, logit, value = total(0), total(1), total(2)
     rate = gap[...] / (1.0 + jnp.exp(logit))
@@ -224,13 +252,13 @@
         return send(sland.at[src], sland.at[src], s_s.at[i], s_r.at[i], (z * group + src, tp))
 
     repeat(group - 1, lambda i: state_copy(i).start())
+    relay(4)
     for cut in cuts:
         scores = dot_on(query_mid[:, cut], key_mid[:, cut], 1, 1)
         scores = jnp.where(below, scores, 0.0).astype(BF16)
         within.append(dot(scores, value[:, cut]))
 
-    for p in range(4, PROJ):
-        project(p)
+    relay(5)
 
     repeat(group - 1, lambda i: state_landing(i).wait_recv())
 
@@ -284,6 +312,34 @@
 
     halo = send(pad.at[pl.ds(length, 8)], pad.at[pl.ds(0, 8)], h_s, h_r, (after, tp))
     halo.start()
+
+    for h in range(heads):
+        sin[:, cuts[h]] = init[h].T
+    for a in range(1, SHARES):
+
+        @pl.when(z >= a)
+        def _():
+            group_landing(a).wait_recv()
+
+    for i in range(SHARES - 1):
+
+        @pl.when(i < z)
+        def _():
+            state, fall = parts_of(gland, i)
+            sin[...] = jnp.exp(fall) * sin[...] + state
+
+    incoming = (jnp.exp(near_decay) * sin[...] + near).astype(BF16)
+    rec = []
+    for h in range(heads):
+        raw = within[h] + dot_on(query_in[:, cuts[h]], incoming[:, cuts[h]], 1, 1)
+        scale = lax.rsqrt(jnp.mean(raw * raw, axis=-1, keepdims=True) + EPS)
+        rec.append((raw * scale * hgain[...]).astype(BF16))
+    rec_out = jnp.concatenate(rec, axis=-1)
+
+    d_out = wof.shape[1]
+    pltpu.make_async_copy(wor, vor, v_l.at[1]).wait()
+    acc[...] = dot(rec_out, vor[...])
+
     gate_out = total(5)
     halo.wait_recv()
     edge = jnp.where(sp > 0, pad[0:8], 0.0)
@@ -295,57 +351,41 @@
         filtered = filtered + taps[j : j + 1] * pad[start : start + length]
     filter_out = (gate_out * filtered).astype(BF16)
 
-    for h in range(heads):
-        sin[:, cuts[h]] = init[h].T
-    for a in range(1, SHARES):
-
-        @pl.when(z >= a)
-        def _():
-            group_landing(a).wait_recv()
-
-    for i in range(SHARES - 1):
-
-        @pl.when(i < z)
-        def _():
-            state, fall = parts_of(gland, i)
-            sin[...] = jnp.exp(fall) * sin[...] + state
-
-    incoming = (jnp.exp(near_decay) * sin[...] + near).astype(BF16)
-    rec = []
-    for h in range(heads):
-        raw = within[h] + dot_on(query_in[:, cuts[h]], incoming[:, cuts[h]], 1, 1)
-        scale = lax.rsqrt(jnp.mean(raw * raw, axis=-1, keepdims=True) + EPS)
-        rec.append((raw * scale * hgain[...]).astype(BF16))
-    rec_out = jnp.concatenate(rec, axis=-1)
-
     pltpu.make_async_copy(wof, vof, v_l.at[0]).wait()
-    pltpu.make_async_copy(wor, vor, v_l.at[1]).wait()
-    d_out = wof.shape[1]
     cols = d_out // CHUNKS
 
-    def out_copy(c, b):
-        to = (sp, shift_t(b))
-        return send(obuf.at[c, shift_t(b)], oland.at[c, b], o_s.at[c, b], o_r.at[c, b], to)
+    def out_copy(c, k):
+        src = (obuf.at[c, corner], obuf.at[c, mate], osend.at[c])[k]
+        to = (sp, across if k == 2 else mate)
+        return send(src, oland.at[c, k], o_s.at[c, k], o_r.at[c, k], to)
+
+    def out_relay(c):
+        out_copy(c, 0).wait_recv()
+        osend[c] = (obuf[c, across].astype(F32) + oland[c, 0].astype(F32)).astype(BF16)
+        out_copy(c, 2).start()
 
     for c in range(CHUNKS):
         cut = slice(c * cols, (c + 1) * cols)
-        part = dot(filter_out, vof[:, cut]) + dot(rec_out, vor[:, cut])
+        part = dot(filter_out, vof[:, cut]) + acc[:, cut]
         obuf[c] = part.astype(BF16).reshape(n_tp, t_loc, cols)
-        for b in range(1, n_tp):
-            out_copy(c, b).start()
+        out_copy(c, 0).start()
+        out_copy(c, 1).start()
+        if c > 0:
+            out_relay(c - 1)
+    out_relay(CHUNKS - 1)
     for c in range(CHUNKS):
         s = obuf[c, tp].astype(F32)
-        for b in range(1, n_tp):
-            out_copy(c, b).wait_recv()
-            s = s + oland[c, b].astype(F32)
+        for k in (1, 2):
+            out_copy(c, k).wait_recv()
+            s = s + oland[c, k].astype(F32)
         out[:, c * cols : (c + 1) * cols] = s.astype(BF16)
 
     for a, b in spread:
         token_copy(a, b).wait_send()
     for p in range(PROJ):
         repeat(group - 1, lambda i: weight_copy(p, i).wait_send())
-        for a in range(1, SHARES):
-            part_copy(p, a).wait_send()
+        for k in range(3):
+            part_copy(p, k).wait_send()
     repeat(group - 1, lambda i: state_copy(i).wait_send())
     for a in range(1, SHARES):
 
@@ -354,8 +394,8 @@
             group_copy(a).wait_send()
 
     for c in range(CHUNKS):
-        for b in range(1, n_tp):
-            out_copy(c, b).wait_send()
+        for k in range(3):
+            out_copy(c, k).wait_send()
 
 
 def body(
@@ -397,14 +437,16 @@
             pltpu.VMEM((SHARES, n_tp, t_loc, depth), BF16),
             pltpu.VMEM((PROJ, depth, width), BF16),
             pltpu.VMEM((PROJ, SHARES, length, width), F32),
-            pltpu.VMEM((PROJ, SHARES, length, width), BF16),
-            pltpu.VMEM((PROJ, SHARES, length, width), BF16),
+            pltpu.VMEM((PROJ, 3, length, width), BF16),
+            pltpu.VMEM((PROJ, 3, length, width), BF16),
             pltpu.VMEM((group, HEAD_DIM + 16, width), BF16),
             pltpu.VMEM((SHARES, HEAD_DIM + 16, width), BF16),
             pltpu.VMEM((HEAD_DIM, width), F32),
             pltpu.VMEM((length + 8, width), F32),
             pltpu.VMEM((CHUNKS, n_tp, t_loc, cols), BF16),
-            pltpu.VMEM((CHUNKS, n_tp, t_loc, cols), BF16),
+            pltpu.VMEM((CHUNKS, 3, t_loc, cols), BF16),
+            pltpu.VMEM((CHUNKS, t_loc, cols), BF16),
+            pltpu.VMEM((length, d_out), F32),
             pltpu.VMEM(w_out_filter.shape, BF16),
             pltpu.VMEM(w_out_rec.shape, BF16),
             dma((SHARES, n_tp)),
@@ -412,16 +454,16 @@
             dma((PROJ,)),
             dma((PROJ, peers)),
             dma((PROJ, peers)),
-            dma((PROJ, SHARES)),
-            dma((PROJ, SHARES)),
+            dma((PROJ, 3)),
+            dma((PROJ, 3)),
             dma((peers,)),
             dma((peers,)),
             dma((SHARES,)),
             dma((SHARES,)),
             dma,
             dma,
-            dma((CHUNKS, n_tp)),
-            dma((CHUNKS, n_tp)),
+            dma((CHUNKS, 3)),
+            dma((CHUNKS, 3)),
             dma((2,)),
         ],
         compiler_params=pltpu.CompilerParams(

time: 70.9 us -> 58.3 us (0.82)
  Pallas kernels: 69.2 us -> 56.6 us
    pallas_call x1, Pallas kernels: 69.2 us -> 56.6 us  [body(): pl.pallas_call(functools.partial(mix_kernel, n_sp, n_tp), out_shape=jax.S...]
where the time goes in v2:
time: 58.3 us; the launch traced here: 58.2 us
  Pallas kernels  56.6 us (97%)
  local copies, waits for them, and re-layouts  1.57 us (3%)
    pallas_call x1, Pallas kernels, body(): pl.pallas_call(functools.partial(mix_kernel, n_sp, n_tp), out_shape=jax.S...  56.6 us
    unnamed x1, local copies, waits for them, and re-layouts  1.57 us

profile of v2, /device:TPU:17, one launch (start us, length us, event | category | flops | bytes accessed | tf_op | source)
XLA Modules:
  0.0 58.2 jit_solution(1579160617565901080)
XLA Ops:
  0.0 56.6 %shard_map.145 = bf16[32,2048]{1,0:T(8,128)(2,1)} custom-call(bf16[32,2048]{1,0:T(8,128)(2,1)} %tok.1, f32[1,2048]{1,0:T(1,128)} %bitcast.3, f32[3,256]{1,0:T(4,128)} %taps.1, f32[1,256]{1,0:T(1,128)} %bitcast.4, f32[128,256]{1,0:T(8,128)} %fade.1, f32[1,128]{1,0:T(1,128)} %bitcast.5, f32[2,128,128]{2,1,0:T(8,128)} %init.1, bf16[256,256]{1,0:T(8,128)(2,1)} %wq.1, ...), custom_call_target="tpu_custom_call" | custom-call | tf_op jit(solution)/shard_map/pallas_call | solution.py:430
  56.6 1.6 %copy.17 = bf16[32,2048]{1,0:T(8,128)(2,1)} copy(bf16[32,2048]{1,0:T(8,128)(2,1)} %shard_map.145) | data formatting | bytes 262144
